TPU v7x, 128 devices: a whole 4x4x4 slice. The times are simulated.
128 devices in a mesh: sp: 64 (over z, y, x), tp: 2 (over core).
Axes of the slice: x: 4, y: 4, z: 4, core: 2. Of those that a mesh axis runs over, the one named last changes fastest.
Arguments:
- queries: bfloat16 [8192, 1024], P('sp', 'tp'), may hold values from -6 to 6
- keys: bfloat16 [8192, 1024], P('sp', 'tp'), may hold values from -6 to 6
- values: bfloat16 [8192, 2048], P('sp', 'tp'), may hold values from -6 to 6
- out_gate: bfloat16 [8192, 2048], P('sp', 'tp'), may hold values from -6 to 6
- decay_rate: float32 [8], P('tp'), may hold values from 0 to 1
- residual: bfloat16 [8192, 2048], P(('sp', 'tp')), may hold values from -6 to 6
- out_weight: bfloat16 [2048, 2048], P('tp'), may hold values from -0.125 to 0.125
- ffn_gain: float32 [2048], replicated, may hold values from 0.1 to 1.9
- route_ids: int32 [8192, 4], P(('sp', 'tp')), may hold values from 0 to 63, all different within a row; in each aligned block of 64 rows (0 to 63, 64 to 127, ...) at most 8 rows name the same one
- route_weights: float32 [8192, 4], P(('sp', 'tp')), may hold values from 0.1 to 1
- gate_up: bfloat16 [64, 2048, 2048], P('sp', None, 'tp'), may hold values from -0.375 to 0.375
- lin_up: bfloat16 [64, 2048, 2048], P('sp', None, 'tp'), may hold values from -0.375 to 0.375
- down_weight: bfloat16 [64, 2048, 2048], P('sp', 'tp'), may hold values from -0.03125 to 0.03125
Outputs:
- layer_out: bfloat16 [8192, 2048], P(('sp', 'tp'))
Inputs may be any that keep to these rules, and one draw needn't show every extreme that they name: `route_ids`: within the rows of one device (aligned blocks of 64 rows), no expert is named by more than 8 entries, a bound that some block reaches; the 4 experts of a row differ.
All inputs are finite; a program needn't handle non-finite values.
Results may differ from a plain program's by a relative error of at most 0.03.
Values may be sent and summed in bfloat16 or wider, within the bound.
A program may use at most 128 MiB of HBM per device.

v0:
```python
import jax
import jax.numpy as jnp
from jax import lax
from jax.sharding import Mesh
from jax.sharding import PartitionSpec as P

D = 2048
DK = 128
DV = 256
SP = ("sp_0", "sp_1", "sp_2")
SP_TP = ("sp_0", "sp_1", "sp_2", "tp")
EPS = 1e-05
CLAMP_LIMIT = 7.0
SIGMOID_SLOPE = 1.702
TOP_PRECISION = lax.Precision.HIGHEST


def carried_state(state_delta, log_gamma, block_len):
    peers, mine = (lax.axis_size(SP), lax.axis_index(SP))
    heads = state_delta.shape[0]
    pieces = state_delta.astype(jnp.bfloat16).reshape(peers, -1)
    arrived = lax.all_to_all(pieces, SP, split_axis=0, concat_axis=0, tiled=True)
    own_log = lax.dynamic_index_in_dim(log_gamma, mine * heads // peers, keepdims=False)
    order = jnp.arange(peers, dtype=jnp.float32)
    gap = order[:, None] - 1.0 - order[None, :]
    weight = jnp.where(gap >= 0, jnp.exp(jnp.maximum(gap, 0.0) * block_len * own_log), 0.0)
    before = jnp.dot(weight, arrived.astype(jnp.float32), precision=TOP_PRECISION)
    returned = lax.all_to_all(
        before.astype(jnp.bfloat16), SP, split_axis=0, concat_axis=0, tiled=True
    )
    return returned.reshape(state_delta.shape).astype(jnp.float32)


def in_blocks(array, dim, peers):
    before, after = (array.shape[:dim], array.shape[dim + 1 :])
    return jnp.moveaxis(array.reshape(*before, peers, -1, *after), dim, 0)


def summed_on_arrival(array, axis, dim):
    tiles = in_blocks(array, dim, lax.axis_size(axis))
    arrived = lax.all_to_all(tiles, axis, split_axis=0, concat_axis=0, tiled=True)
    return arrived.astype(jnp.float32).sum(axis=0)


def expert_act(row_block, gate_part, lin_part):
    gate_pre = jnp.dot(row_block, gate_part, preferred_element_type=jnp.float32)
    lin_pre = jnp.dot(row_block, lin_part, preferred_element_type=jnp.float32)
    gate_clip = jnp.minimum(gate_pre, CLAMP_LIMIT)
    lin_clip = jnp.clip(lin_pre, -CLAMP_LIMIT, CLAMP_LIMIT)
    return (gate_clip * jax.nn.sigmoid(SIGMOID_SLOPE * gate_clip) * (lin_clip + 1.0)).astype(
        jnp.bfloat16
    )


def local(
    queries,
    keys,
    values,
    out_gate,
    decay_rate,
    residual,
    out_weight,
    ffn_gain,
    route_ids,
    route_weights,
    gate_up,
    lin_up,
    down_weight,
):
    block_len = queries.shape[0]
    local_heads = decay_rate.shape[0]
    log_gamma = -decay_rate
    query_heads = queries.astype(jnp.float32).reshape(block_len, local_heads, DK).transpose(1, 0, 2)
    per_head_keys = keys.astype(jnp.float32).reshape(block_len, local_heads, DK).transpose(
        1, 0, 2
    ) * DK ** (-0.5)
    per_head_values = (
        values.astype(jnp.float32).reshape(block_len, local_heads, DV).transpose(1, 0, 2)
    )
    positions = jnp.arange(block_len, dtype=jnp.float32)
    offsets = positions[:, None] - positions[None, :]
    causal = offsets >= 0
    decay_mask = jnp.where(
        causal[None], jnp.exp(jnp.where(causal, offsets, 0.0)[None] * log_gamma[:, None, None]), 0.0
    )
    trailing_decay = jnp.exp((block_len - 1.0 - positions)[None, :] * log_gamma[:, None])
    lead_decay = jnp.exp((positions + 1.0)[None, :] * log_gamma[:, None])
    attention_scores = (
        jnp.einsum("hqd,hkd->hqk", query_heads, per_head_keys, precision=TOP_PRECISION) * decay_mask
    )
    intra_block_term = jnp.einsum(
        "zfp,zpn->zfn", attention_scores, per_head_values, precision=TOP_PRECISION
    )
    state_delta = jnp.einsum(
        "mxs,mxq->msq",
        per_head_keys * trailing_decay[:, :, None],
        per_head_values,
        precision=TOP_PRECISION,
    )
    carried = carried_state(state_delta, log_gamma, block_len)
    cross_term = (
        jnp.einsum("hqd,hdv->hqv", query_heads, carried, precision=TOP_PRECISION)
        * lead_decay[:, :, None]
    )
    retained = intra_block_term + cross_term
    normed = retained * lax.rsqrt(jnp.mean(retained * retained, axis=-1, keepdims=True) + EPS)
    gated = (
        normed.transpose(1, 0, 2).reshape(block_len, local_heads * DV)
        * jax.nn.silu(out_gate.astype(jnp.float32))
    ).astype(jnp.bfloat16)
    mix_rows = summed_on_arrival(
        jnp.dot(gated, out_weight, preferred_element_type=jnp.float32).astype(jnp.bfloat16), "tp", 0
    )
    mixed = (residual.astype(jnp.float32) + mix_rows).astype(jnp.bfloat16)
    mixed_wide = mixed.astype(jnp.float32)
    normed_rows = (
        mixed_wide
        * lax.rsqrt(jnp.mean(mixed_wide * mixed_wide, axis=-1, keepdims=True) + EPS)
        * ffn_gain
    ).astype(jnp.bfloat16)
    experts = lax.axis_size(SP)
    own_rows = route_ids.shape[0]
    top_count = route_ids.shape[1]
    capacity = own_rows * top_count * lax.axis_size("tp") // experts
    flat_ids = route_ids.reshape(-1)
    one_hot = (flat_ids[:, None] == jnp.arange(experts, dtype=jnp.int32)[None, :]).astype(jnp.int32)
    slot_rank = jnp.sum(one_hot * (jnp.cumsum(one_hot, axis=0) - 1), axis=1)
    slot_index = flat_ids * capacity + slot_rank
    source_row = jnp.arange(own_rows * top_count, dtype=jnp.int32) // top_count
    slot_source = (
        jnp.full((experts * capacity,), own_rows, jnp.int32).at[slot_index].set(source_row)
    )
    padded = jnp.concatenate([normed_rows, jnp.zeros((1, D), jnp.bfloat16)], axis=0)
    outgoing = padded[slot_source].reshape(experts, capacity, D)
    gate_half = gate_up[0]
    lin_half = lin_up[0]
    down_half = down_weight[0]
    pair_rows = lax.all_gather(
        lax.all_to_all(outgoing, SP, split_axis=0, concat_axis=0, tiled=True),
        "tp",
        axis=0,
        tiled=True,
    )
    activation = expert_act(pair_rows.reshape(-1, D), gate_half, lin_half)
    partial_value = jnp.dot(activation, down_half, preferred_element_type=jnp.float32).reshape(
        pair_rows.shape
    )
    summed = summed_on_arrival(partial_value.astype(jnp.bfloat16), "tp", 0)
    returned = lax.all_to_all(
        summed.astype(jnp.bfloat16), SP, split_axis=0, concat_axis=0, tiled=True
    )
    picked = (
        returned.reshape(experts * capacity, D)[slot_index]
        .reshape(own_rows, top_count, D)
        .astype(jnp.float32)
    )
    expert_sum = jnp.sum(picked * route_weights[:, :, None], axis=1)
    return (mixed_wide + expert_sum).astype(jnp.bfloat16)


def solution(mesh):
    torus = Mesh(mesh.devices.reshape(4, 4, 4, mesh.shape["tp"]), ("sp_0", "sp_1", "sp_2", "tp"))
    in_specs = (
        P(SP, "tp"),
        P(SP, "tp"),
        P(SP, "tp"),
        P(SP, "tp"),
        P("tp"),
        P(SP_TP, None),
        P("tp", None),
        P(),
        P(SP_TP, None),
        P(SP_TP, None),
        P(SP, None, "tp"),
        P(SP, None, "tp"),
        P(SP, "tp", None),
    )
    out_specs = P(SP_TP, None)
    return jax.shard_map(local, mesh=torus, in_specs=in_specs, out_specs=out_specs, check_vma=False)
```

profile of v0, /device:TPU:0, one launch (start us, length us, event | category | flops | bytes accessed | tf_op | source)
XLA Modules:
  0.0 202.1 jit_solution(13798051839371577354)
XLA Ops:
  6.5 0.7 neg.10
  7.3 1.0 copy.102
  8.3 1.3 convolution_convert_fusion.2
  9.8 0.6 broadcast.223
  10.4 2.2 %reduce.4 = bf16[64,2048]{1,0:T(8,128)(2,1)S(1)} reduce(bf16[64,1,2048]{2,1,0:T(2,128)(2,1)S(1)} %all_to_all.35, bf16[]{:T(256)} %broadcast.223), dimensions={1}, to_apply=%all_to_all.35.reduce_sub_computation | reduce | bytes 524290 | tf_op jit(solution)/shard_map/all_to_all | solution.py:22
  12.6 0.9 reshape.247
  13.5 11.7 %all-to-all-start = ((bf16[64,2,1024]{2,1,0:T(2,128)(2,1)}), bf16[64,2,1024]{2,1,0:T(2,128)(2,1)S(1)}, u32[]{:S(2)}, u32[]{:S(2)}) async-start(bf16[64,2,1024]{2,1,0:T(2,128)(2,1)} %reshape.247), calls=%async_computation | async-start | bytes 524288 | tf_op jit(solution)/shard_map/all_to_all | solution.py:22
  25.3 0.8 copy.90
  26.3 0.7 broadcast_multiply_fusion
  27.0 0.6 reduce-window.6
  27.6 0.2 slice_reduce_fusion
  28.2 0.6 dynamic_slice.4
  29.3 1.4 scatter_custom_fusion
  30.8 5.0 %all-to-all-done = bf16[64,2,1024]{2,1,0:T(2,128)(2,1)S(1)} async-done(((bf16[64,2,1024]{2,1,0:T(2,128)(2,1)}), bf16[64,2,1024]{2,1,0:T(2,128)(2,1)S(1)}, u32[]{:S(2)}, u32[]{:S(2)}) %all-to-all-start) | async-done | bytes 262176 | tf_op jit(solution)/shard_map/all_to_all | solution.py:22
  35.8 0.2 reshape.248
  36.0 0.5 fusion.11
  36.5 0.8 reduce.5
  37.3 0.9 reshape.249
  38.2 5.4 %all-to-all-start.1 = ((bf16[64,2,1024]{2,1,0:T(2,128)(2,1)}), bf16[64,2,1024]{2,1,0:T(2,128)(2,1)S(1)}, u32[]{:S(2)}, u32[]{:S(2)}) async-start(bf16[64,2,1024]{2,1,0:T(2,128)(2,1)} %reshape.249), calls=%async_computation.1 | async-start | bytes 524288 | tf_op jit(solution)/shard_map/all_to_all | solution.py:28
  43.6 0.2 copy.88
  43.8 0.4 fusion.22
  44.2 10.0 %all-to-all-done.1 = bf16[64,2,1024]{2,1,0:T(2,128)(2,1)S(1)} async-done(((bf16[64,2,1024]{2,1,0:T(2,128)(2,1)}), bf16[64,2,1024]{2,1,0:T(2,128)(2,1)S(1)}, u32[]{:S(2)}, u32[]{:S(2)}) %all-to-all-start.1) | async-done | bytes 262176 | tf_op jit(solution)/shard_map/all_to_all | solution.py:28
  54.2 0.2 reshape.250
  54.4 1.5 reduce.1
  56.0 0.2 fusion.43
  56.3 0.5 fusion.32
  56.8 0.2 fusion.34
  57.0 0.2 copy.87
  57.4 2.9 %convolution_convert_fusion = bf16[128,2048]{1,0:T(8,128)(2,1)S(1)} fusion(bf16[128,1024]{0,1:T(8,128)(2,1)S(1)} %fusion.35, bf16[1024,2048]{1,0:T(8,128)(2,1)} %param.19), kind=kOutput, calls=%fused_computation.13 | convolution fusion | flops 537133056 | bytes 4980736 | tf_op jit(solution)/shard_map/dot_general | solution.py:112
  60.3 4.2 %all_to_all.42 = bf16[2,64,2048]{2,1,0:T(8,128)(2,1)S(1)} all-to-all(bf16[2,64,2048]{2,1,0:T(8,128)(2,1)S(1)} %bitcast.118), channel_id=1, replica_groups=mesh['sp_0'=4,'sp_1'=4,'sp_2'=4,'tp'=2] {'tp'}, dimensions={0} | all-to-all | bytes 1048576 | tf_op jit(solution)/shard_map/all_to_all | solution.py:41
  64.6 0.2 fusion.27
  65.0 2.5 %gather_fusion = bf16[512,2048]{1,0:T(8,128)(2,1)S(1)} fusion(bf16[65,2048]{1,0:T(8,128)(2,1)S(1)} %concatenate.3, s32[1024]{0:T(1024)S(1)} %pad_clamp_fusion.1), kind=kCustom, calls=%fused_computation | custom fusion | bytes 4196352 | tf_op jit(solution)/shard_map/gather | solution.py:134
  67.4 35.2 %all_to_all.43 = bf16[64,8,2048]{2,1,0:T(8,128)(2,1)} all-to-all(bf16[64,8,2048]{2,1,0:T(8,128)(2,1)S(1)} %bitcast.114), channel_id=1, replica_groups=mesh['sp_0'=4,'sp_1'=4,'sp_2'=4,'tp'=2] {'sp_0','sp_1','sp_2'}, dimensions={0} | all-to-all | bytes 4194304 | tf_op jit(solution)/shard_map/all_to_all | solution.py:139
  102.7 13.1 %all-gather.2.cloned.1.call-done = bf16[128,8,2048]{2,1,0:T(8,128)(2,1)} async-done(((bf16[64,8,2048]{2,1,0:T(8,128)(2,1)}), bf16[128,8,2048]{2,1,0:T(8,128)(2,1)}) %all-gather.2.cloned.1.call-update) | async-done | bytes 4194320 | tf_op jit(solution)/shard_map/all_gather | solution.py:138
  115.8 7.6 %fusion.2 = f32[1024,1024]{1,0:T(8,128)S(1)} fusion(bf16[1,2048,1024]{2,1,0:T(8,128)(2,1)} %param.24, bf16[128,8,2048]{2,1,0:T(8,128)(2,1)} %all-gather.2.cloned.1.call-done), kind=kOutput, calls=%fused_computation.5 | convolution fusion | flops 4294967296 | bytes 12582912 | tf_op jit(solution)/shard_map/dot_general | solution.py:47
  123.5 5.8 %fusion.17 = bf16[128,8,1024]{2,1,0:T(8,128)(2,1)S(1)} fusion(f32[1024,1024]{1,0:T(8,128)S(1)} %fusion.2, bf16[1,2048,1024]{2,1,0:T(8,128)(2,1)S(1)} %copy-done.6, bf16[128,8,2048]{2,1,0:T(8,128)(2,1)S(1)} %copy-done.8), kind=kOutput, calls=%fused_computation.18 | convolution fusion | flops 4305453056 | bytes 14680064 | tf_op jit(solution)/shard_map/dot_general | solution.py:46
  129.3 5.2 %fusion.8 = bf16[128,8,2048]{2,0,1:T(8,128)(2,1)S(1)} fusion(bf16[1,1024,2048]{2,1,0:T(8,128)(2,1)S(1)} %copy-done.7, bf16[128,8,1024]{2,1,0:T(8,128)(2,1)S(1)} %fusion.17), kind=kOutput, calls=%fused_computation.12 | convolution fusion | flops 4297064448 | bytes 10485760 | tf_op jit(solution)/shard_map/dot_general | solution.py:145
  134.5 0.6 copy.94
  135.1 8.2 %all_to_all.44 = bf16[2,64,8,2048]{3,1,2,0:T(8,128)(2,1)} all-to-all(bf16[2,64,8,2048]{3,1,2,0:T(8,128)(2,1)S(1)} %copy.94), channel_id=1, replica_groups=mesh['sp_0'=4,'sp_1'=4,'sp_2'=4,'tp'=2] {'tp'}, dimensions={0} | all-to-all | bytes 8388608 | tf_op jit(solution)/shard_map/all_to_all | solution.py:41
  143.2 3.5 %reduce_sum.64 = bf16[64,8,2048]{2,0,1:T(8,128)(2,1)S(1)} reduce(bf16[2,64,8,2048]{3,1,2,0:T(8,128)(2,1)} %all_to_all.44, bf16[]{:T(256)} %constant.96.clone.1), dimensions={0}, to_apply=%region_7.8 | reduce | flops 1048576 | bytes 6291458 | tf_op jit(solution)/shard_map/reduce_sum | solution.py:42
  146.7 2.5 %copy.96 = bf16[64,8,2048]{2,1,0:T(8,128)(2,1)} copy(bf16[64,8,2048]{2,0,1:T(8,128)(2,1)S(1)} %reduce_sum.64) | data formatting | bytes 4194304 | tf_op jit(solution)/shard_map/reduce_sum | solution.py:42
  149.2 10.6 %all-to-all-start.5 = ((bf16[64,8,2048]{2,1,0:T(8,128)(2,1)}), bf16[64,8,2048]{2,1,0:T(8,128)(2,1)S(1)}, u32[]{:S(2)}, u32[]{:S(2)}) async-start(bf16[64,8,2048]{2,1,0:T(8,128)(2,1)} %copy.96), calls=%async_computation.5 | async-start | bytes 4194304 | tf_op jit(solution)/shard_map/all_to_all | solution.py:149
  159.9 0.7 copy.97
  160.6 29.4 %all-to-all-done.5 = bf16[64,8,2048]{2,1,0:T(8,128)(2,1)S(1)} async-done(((bf16[64,8,2048]{2,1,0:T(8,128)(2,1)}), bf16[64,8,2048]{2,1,0:T(8,128)(2,1)S(1)}, u32[]{:S(2)}, u32[]{:S(2)}) %all-to-all-start.5) | async-done | bytes 2097184 | tf_op jit(solution)/shard_map/all_to_all | solution.py:149
  190.0 1.4 gather_fusion.1
  191.4 0.7 reshape.215
  192.1 2.4 %multiply_reduce_fusion = f32[64,2048]{1,0:T(8,128)S(1)} fusion(f32[64,4,2048]{2,1,0:T(4,128)S(1)} %reshape.215, f32[64,4]{1,0:T(8,128)} %copy.97), kind=kLoop, calls=%fused_computation.17 | loop fusion | flops 917504 | bytes 2622464 | tf_op jit(solution)/shard_map/reduce_sum | solution.py:157
  194.5 0.8 fusion.30
  (47 shorter events, 1.6 us)
Async XLA Ops:
  6.5 37.3 %copy-start = (bf16[128,512]{1,0:T(8,128)(2,1)S(1)}, bf16[128,512]{1,0:T(8,128)(2,1)}, u32[]{:S(2)}) copy-start(bf16[128,512]{1,0:T(8,128)(2,1)} %param.13) | copy-start | bytes 393220
  6.5 37.1 %copy-start.2 = (bf16[128,1024]{1,0:T(8,128)(2,1)S(1)}, bf16[128,1024]{1,0:T(8,128)(2,1)}, u32[]{:S(2)}) copy-start(bf16[128,1024]{1,0:T(8,128)(2,1)} %param.16) | copy-start | bytes 786436
  13.5 42.8 %copy-start.1 = (bf16[128,1024]{1,0:T(8,128)(2,1)S(1)}, bf16[128,1024]{1,0:T(8,128)(2,1)}, u32[]{:S(2)}) copy-start(bf16[128,1024]{1,0:T(8,128)(2,1)} %param.15) | copy-start | bytes 786436
  13.5 22.3 %all-to-all-start = ((bf16[64,2,1024]{2,1,0:T(2,128)(2,1)}), bf16[64,2,1024]{2,1,0:T(2,128)(2,1)S(1)}, u32[]{:S(2)}, u32[]{:S(2)}) async-start(bf16[64,2,1024]{2,1,0:T(2,128)(2,1)} %reshape.247), calls=%async_computation | async-start | bytes 524288 | tf_op jit(solution)/shard_map/all_to_all | solution.py:22
  38.2 16.0 %all-to-all-start.1 = ((bf16[64,2,1024]{2,1,0:T(2,128)(2,1)}), bf16[64,2,1024]{2,1,0:T(2,128)(2,1)S(1)}, u32[]{:S(2)}, u32[]{:S(2)}) async-start(bf16[64,2,1024]{2,1,0:T(2,128)(2,1)} %reshape.249), calls=%async_computation.1 | async-start | bytes 524288 | tf_op jit(solution)/shard_map/all_to_all | solution.py:28
  43.5 72.3 %all-gather.2.cloned.1.call-start = ((), (), s32[]{:S(2)}) async-start(), calls=%async_computation.6 | async-start | bytes 6291456 | tf_op jit(solution)/shard_map/all_gather | solution.py:138
  57.2 7.4 %copy-start.3 = (bf16[64,2048]{1,0:T(8,128)(2,1)S(1)}, bf16[64,2048]{1,0:T(8,128)(2,1)}, u32[]{:S(2)}) copy-start(bf16[64,2048]{1,0:T(8,128)(2,1)} %param.18) | copy-start | bytes 786436
  57.4 7.4 %copy-start.4 = (f32[2048]{0:T(1024)S(1)}, f32[2048]{0:T(1024)}, u32[]{:S(2)}) copy-start(f32[2048]{0:T(1024)} %param.20) | copy-start | bytes 24580
  115.8 7.7 %copy-start.6 = (bf16[1,2048,1024]{2,1,0:T(8,128)(2,1)S(1)}, bf16[1,2048,1024]{2,1,0:T(8,128)(2,1)}, u32[]{:S(2)}) copy-start(bf16[1,2048,1024]{2,1,0:T(8,128)(2,1)} %param.23) | copy-start | bytes 12582916
  115.8 7.7 %copy-start.8 = (bf16[128,8,2048]{2,1,0:T(8,128)(2,1)S(1)}, bf16[128,8,2048]{2,1,0:T(8,128)(2,1)}, u32[]{:S(2)}) copy-start(bf16[128,8,2048]{2,1,0:T(8,128)(2,1)} %all-gather.2.cloned.1.call-done) | copy-start | bytes 12582916
  123.5 5.8 %copy-start.7 = (bf16[1,1024,2048]{2,1,0:T(8,128)(2,1)S(1)}, bf16[1,1024,2048]{2,1,0:T(8,128)(2,1)}, u32[]{:S(2)}) copy-start(bf16[1,1024,2048]{2,1,0:T(8,128)(2,1)} %param.25) | copy-start | bytes 12582916
  146.7 13.1 %copy-start.5 = (f32[64,4]{0,1:T(4,128)S(1)}, f32[64,4]{0,1:T(4,128)}, u32[]{:S(2)}) copy-start(f32[64,4]{0,1:T(4,128)} %param.22) | copy-start | bytes 3076
  149.2 40.8 %all-to-all-start.5 = ((bf16[64,8,2048]{2,1,0:T(8,128)(2,1)}), bf16[64,8,2048]{2,1,0:T(8,128)(2,1)S(1)}, u32[]{:S(2)}, u32[]{:S(2)}) async-start(bf16[64,8,2048]{2,1,0:T(8,128)(2,1)} %copy.96), calls=%async_computation.5 | async-start | bytes 4194304 | tf_op jit(solution)/shard_map/all_to_all | solution.py:149
Sparse Core Ops, SparseCore 0:
  102.8 12.9 all-gather.1
where the time goes:
time: 203 us; the launch traced here: 202 us
  waiting for transfers between devices  57.5 us (28%)
  blocking collectives  47.6 us (23%)
  starting transfers between devices  27.7 us (14%)
  matrix products  24.4 us (12%)
  local copies, waits for them, and re-layouts  16.2 us (8%)
  between operations  14.4 us (7%)
  other arithmetic  14.3 us (7%)
    all_to_all x1, blocking collectives, local(): lax.all_to_all(outgoing, SP, split_axis=0, concat_axis=0, tiled=True)  35.2 us
    all_to_all x1, waiting for transfers between devices, local(): lax.all_to_all(summed.astype(jnp.bfloat16), SP, split_axis=0, concat_axis...  29.4 us
    all_gather x1, waiting for transfers between devices, local(): lax.all_gather(lax.all_to_all(outgoing, SP, split_axis=0, concat_axis=0,...  13.1 us
    all_to_all x2, blocking collectives, summed_on_arrival(): lax.all_to_all(tiles, axis, split_axis=0, concat_axis=0, tiled=True)  12.3 us
    all_to_all x1, starting transfers between devices, carried_state(): lax.all_to_all(pieces, SP, split_axis=0, concat_axis=0, tiled=True)  11.7 us
    all_to_all x1, starting transfers between devices, local(): lax.all_to_all(summed.astype(jnp.bfloat16), SP, split_axis=0, concat_axis...  10.6 us
    all_to_all x1, waiting for transfers between devices, carried_state(): lax.all_to_all(before.astype(jnp.bfloat16), SP, split_axis=0, concat_axis...  9.95 us
    dot_general x1, matrix products, expert_act(): lin_pre = jnp.dot(row_block, lin_part, preferred_element_type=jnp.float32)  7.65 us
  transfers between devices with their start and end apart: 4, of which 4 were waited for; matrix products, arithmetic and copies ran while one was open for 3% of the time, Pallas kernels for 0%

commit v1 on v0

--- a/solution.py
+++ b/solution.py
@@ -13,6 +13,12 @@
 CLAMP_LIMIT = 7.0
 SIGMOID_SLOPE = 1.702
 TOP_PRECISION = lax.Precision.HIGHEST
+
+
+def tiled_gather(x, axis, dim):
+    size = lax.axis_size(axis)
+    repeats = [size if d == dim else 1 for d in range(x.ndim)]
+    return lax.all_to_all(jnp.tile(x, repeats), axis, split_axis=dim, concat_axis=dim, tiled=True)
 
 
 def carried_state(state_delta, log_gamma, block_len):
@@ -135,11 +141,8 @@
     gate_half = gate_up[0]
     lin_half = lin_up[0]
     down_half = down_weight[0]
-    pair_rows = lax.all_gather(
-        lax.all_to_all(outgoing, SP, split_axis=0, concat_axis=0, tiled=True),
-        "tp",
-        axis=0,
-        tiled=True,
+    pair_rows = tiled_gather(
+        lax.all_to_all(outgoing, SP, split_axis=0, concat_axis=0, tiled=True), "tp", 0
     )
     activation = expert_act(pair_rows.reshape(-1, D), gate_half, lin_half)
     partial_value = jnp.dot(activation, down_half, preferred_element_type=jnp.float32).reshape(

time: 203 us -> 176 us (0.87)
  between operations: 14.4 us -> 1.02 us
  waiting for transfers between devices: 57.5 us -> 44.8 us
  blocking collectives: 47.6 us -> 54.8 us
  starting transfers between devices: 27.7 us -> 22.7 us
  matrix products: 24.4 us -> 21.4 us
    all_gather x1 -> x0, waiting for transfers between devices: 13.1 us -> none  [local(): lax.all_gather(lax.all_to_all(outgoing, SP, split_axis=0, concat_axis=0,...]
    all_to_all x0 -> x1, blocking collectives: none -> 7.37 us  [tiled_gather(): lax.all_to_all(jnp.tile(x, repeats), axis, split_axis=dim, concat_axis=di...]
    all_to_all x1, starting transfers between devices: 10.6 us -> 5.68 us  [local(): lax.all_to_all(summed.astype(jnp.bfloat16), SP, split_axis=0, concat_axis...]
    dot_general x1, matrix products: 7.65 us -> 4.54 us  [expert_act(): lin_pre = jnp.dot(row_block, lin_part, preferred_element_type=jnp.float32)]
  transfers between devices with their start and end apart: 4 -> 3, of which waited for: 4 -> 3; matrix products, arithmetic and copies ran while one was open for 3% -> 4% of each run, Pallas kernels for 0% -> 0%
where the time goes in v1:
time: 176 us
  blocking collectives  54.8 us (31%)
  waiting for transfers between devices  44.8 us (25%)
  starting transfers between devices  22.7 us (13%)
  matrix products  21.4 us (12%)
  local copies, waits for them, and re-layouts  16.7 us (9%)
  other arithmetic  14.2 us (8%)
    all_to_all x1, blocking collectives, local(): lax.all_to_all(outgoing, SP, split_axis=0, concat_axis=0, tiled=True)  35.1 us
    all_to_all x1, waiting for transfers between devices, local(): lax.all_to_all(summed.astype(jnp.bfloat16), SP, split_axis=0, concat_axis...  29.8 us
    all_to_all x2, blocking collectives, summed_on_arrival(): lax.all_to_all(tiles, axis, split_axis=0, concat_axis=0, tiled=True)  12.3 us
    all_to_all x1, starting transfers between devices, carried_state(): lax.all_to_all(pieces, SP, split_axis=0, concat_axis=0, tiled=True)  11.7 us
    all_to_all x1, waiting for transfers between devices, carried_state(): lax.all_to_all(before.astype(jnp.bfloat16), SP, split_axis=0, concat_axis...  10 us
    all_to_all x1, blocking collectives, tiled_gather(): lax.all_to_all(jnp.tile(x, repeats), axis, split_axis=dim, concat_axis=di...  7.37 us
    dot_general x1, matrix products, expert_act(): gate_pre = jnp.dot(row_block, gate_part, preferred_element_type=jnp.float32)  5.77 us
    all_to_all x1, starting transfers between devices, local(): lax.all_to_all(summed.astype(jnp.bfloat16), SP, split_axis=0, concat_axis...  5.68 us
  transfers between devices with their start and end apart: 3, of which 3 were waited for; matrix products, arithmetic and copies ran while one was open for 4% of the time, Pallas kernels for 0%

profile of v1, /device:TPU:0, one launch (start us, length us, event | category | flops | bytes accessed | tf_op | source)
XLA Modules:
  0.0 175.6 jit_solution(7799539435737695797)
XLA Ops:
  0.0 0.7 neg.10
  0.7 1.0 copy.102
  1.8 1.3 convolution_convert_fusion.2
  3.3 0.6 broadcast.226
  3.9 2.2 %reduce.4 = bf16[64,2048]{1,0:T(8,128)(2,1)S(1)} reduce(bf16[64,1,2048]{2,1,0:T(2,128)(2,1)S(1)} %all_to_all.39, bf16[]{:T(256)} %broadcast.226), dimensions={1}, to_apply=%all_to_all.39.reduce_sub_computation | reduce | bytes 524290 | tf_op jit(solution)/shard_map/all_to_all | solution.py:28
  6.1 0.9 reshape.251
  7.0 11.7 %all-to-all-start = ((bf16[64,2,1024]{2,1,0:T(2,128)(2,1)}), bf16[64,2,1024]{2,1,0:T(2,128)(2,1)S(1)}, u32[]{:S(2)}, u32[]{:S(2)}) async-start(bf16[64,2,1024]{2,1,0:T(2,128)(2,1)} %reshape.251), calls=%async_computation | async-start | bytes 524288 | tf_op jit(solution)/shard_map/all_to_all | solution.py:28
  18.8 0.8 copy.90
  19.8 0.7 broadcast_multiply_fusion
  20.5 0.6 reduce-window.6
  21.1 0.2 slice_reduce_fusion
  21.7 0.6 dynamic_slice.4
  22.8 1.4 scatter_custom_fusion
  24.2 5.0 %all-to-all-done = bf16[64,2,1024]{2,1,0:T(2,128)(2,1)S(1)} async-done(((bf16[64,2,1024]{2,1,0:T(2,128)(2,1)}), bf16[64,2,1024]{2,1,0:T(2,128)(2,1)S(1)}, u32[]{:S(2)}, u32[]{:S(2)}) %all-to-all-start) | async-done | bytes 262176 | tf_op jit(solution)/shard_map/all_to_all | solution.py:28
  29.2 0.2 reshape.252
  29.5 0.5 fusion.11
  29.9 0.8 reduce.5
  30.8 0.9 reshape.253
  31.6 5.4 %all-to-all-start.1 = ((bf16[64,2,1024]{2,1,0:T(2,128)(2,1)}), bf16[64,2,1024]{2,1,0:T(2,128)(2,1)S(1)}, u32[]{:S(2)}, u32[]{:S(2)}) async-start(bf16[64,2,1024]{2,1,0:T(2,128)(2,1)} %reshape.253), calls=%async_computation.1 | async-start | bytes 524288 | tf_op jit(solution)/shard_map/all_to_all | solution.py:34
  37.2 0.4 fusion.22
  37.6 10.0 %all-to-all-done.1 = bf16[64,2,1024]{2,1,0:T(2,128)(2,1)S(1)} async-done(((bf16[64,2,1024]{2,1,0:T(2,128)(2,1)}), bf16[64,2,1024]{2,1,0:T(2,128)(2,1)S(1)}, u32[]{:S(2)}, u32[]{:S(2)}) %all-to-all-start.1) | async-done | bytes 262176 | tf_op jit(solution)/shard_map/all_to_all | solution.py:34
  47.6 0.2 reshape.254
  47.8 1.5 reduce.1
  49.5 0.2 fusion.43
  49.7 0.5 fusion.32
  50.3 0.2 fusion.34
  50.5 0.2 copy.87
  50.9 2.9 %convolution_convert_fusion = bf16[128,2048]{1,0:T(8,128)(2,1)S(1)} fusion(bf16[128,1024]{0,1:T(8,128)(2,1)S(1)} %fusion.35, bf16[1024,2048]{1,0:T(8,128)(2,1)} %param.19), kind=kOutput, calls=%fused_computation.13 | convolution fusion | flops 537133056 | bytes 4980736 | tf_op jit(solution)/shard_map/dot_general | solution.py:118
  53.8 4.2 %all_to_all.47 = bf16[2,64,2048]{2,1,0:T(8,128)(2,1)S(1)} all-to-all(bf16[2,64,2048]{2,1,0:T(8,128)(2,1)S(1)} %bitcast.120), channel_id=1, replica_groups=mesh['sp_0'=4,'sp_1'=4,'sp_2'=4,'tp'=2] {'tp'}, dimensions={0} | all-to-all | bytes 1048576 | tf_op jit(solution)/shard_map/all_to_all | solution.py:47
  58.1 0.2 fusion.27
  58.4 2.5 %gather_fusion = bf16[512,2048]{1,0:T(8,128)(2,1)S(1)} fusion(bf16[65,2048]{1,0:T(8,128)(2,1)S(1)} %concatenate.3, s32[1024]{0:T(1024)S(1)} %pad_clamp_fusion.1), kind=kCustom, calls=%fused_computation | custom fusion | bytes 4196352 | tf_op jit(solution)/shard_map/gather | solution.py:140
  60.9 35.1 %all_to_all.48 = bf16[64,8,2048]{2,1,0:T(8,128)(2,1)S(1)} all-to-all(bf16[64,8,2048]{2,1,0:T(8,128)(2,1)S(1)} %bitcast.116), channel_id=1, replica_groups=mesh['sp_0'=4,'sp_1'=4,'sp_2'=4,'tp'=2] {'sp_0','sp_1','sp_2'}, dimensions={0} | all-to-all | bytes 4194304 | tf_op jit(solution)/shard_map/all_to_all | solution.py:145
  96.0 0.5 tile.4
  96.6 7.4 %all_to_all.49 = bf16[128,8,2048]{2,1,0:T(8,128)(2,1)S(1)} all-to-all(bf16[128,8,2048]{2,1,0:T(8,128)(2,1)S(1)} %bitcast.115), channel_id=1, replica_groups=mesh['sp_0'=4,'sp_1'=4,'sp_2'=4,'tp'=2] {'tp'}, dimensions={0} | all-to-all | bytes 8388608 | tf_op jit(solution)/shard_map/all_to_all | solution.py:21
  103.9 4.5 %fusion.2 = f32[1024,1024]{1,0:T(8,128)S(1)} fusion(bf16[1,2048,1024]{2,1,0:T(8,128)(2,1)S(1)} %copy-done.7, bf16[128,8,2048]{2,1,0:T(8,128)(2,1)S(1)} %all_to_all.49), kind=kOutput, calls=%fused_computation.5 | convolution fusion | flops 4294967296 | bytes 12582912 | tf_op jit(solution)/shard_map/dot_general | solution.py:53
  108.5 5.8 %fusion.17 = bf16[128,8,1024]{2,1,0:T(8,128)(2,1)S(1)} fusion(f32[1024,1024]{1,0:T(8,128)S(1)} %fusion.2, bf16[1,2048,1024]{2,1,0:T(8,128)(2,1)S(1)} %copy-done.8, bf16[128,8,2048]{2,1,0:T(8,128)(2,1)S(1)} %all_to_all.49), kind=kOutput, calls=%fused_computation.18 | convolution fusion | flops 4305453056 | bytes 14680064 | tf_op jit(solution)/shard_map/dot_general | solution.py:52
  114.3 5.2 %fusion.8 = bf16[128,8,2048]{2,0,1:T(8,128)(2,1)S(1)} fusion(bf16[1,1024,2048]{2,1,0:T(8,128)(2,1)S(1)} %copy-done.9, bf16[128,8,1024]{2,1,0:T(8,128)(2,1)S(1)} %fusion.17), kind=kOutput, calls=%fused_computation.12 | convolution fusion | flops 4297064448 | bytes 10485760 | tf_op jit(solution)/shard_map/dot_general | solution.py:148
  119.5 0.6 copy.94
  120.1 8.2 %all_to_all.50 = bf16[2,64,8,2048]{3,1,2,0:T(8,128)(2,1)} all-to-all(bf16[2,64,8,2048]{3,1,2,0:T(8,128)(2,1)S(1)} %copy.94), channel_id=1, replica_groups=mesh['sp_0'=4,'sp_1'=4,'sp_2'=4,'tp'=2] {'tp'}, dimensions={0} | all-to-all | bytes 8388608 | tf_op jit(solution)/shard_map/all_to_all | solution.py:47
  128.3 3.5 %reduce_sum.64 = bf16[64,8,2048]{2,0,1:T(8,128)(2,1)S(1)} reduce(bf16[2,64,8,2048]{3,1,2,0:T(8,128)(2,1)} %all_to_all.50, bf16[]{:T(256)} %constant.96.clone.1), dimensions={0}, to_apply=%region_7.8 | reduce | flops 1048576 | bytes 6291458 | tf_op jit(solution)/shard_map/reduce_sum | solution.py:48
  131.8 2.5 %copy.96 = bf16[64,8,2048]{2,1,0:T(8,128)(2,1)} copy(bf16[64,8,2048]{2,0,1:T(8,128)(2,1)S(1)} %reduce_sum.64) | data formatting | bytes 4194304 | tf_op jit(solution)/shard_map/reduce_sum | solution.py:48
  134.3 5.7 %all-to-all-start.6 = ((bf16[64,8,2048]{2,1,0:T(8,128)(2,1)}), bf16[64,8,2048]{2,1,0:T(8,128)(2,1)S(1)}, u32[]{:S(2)}, u32[]{:S(2)}) async-start(bf16[64,8,2048]{2,1,0:T(8,128)(2,1)} %copy.96), calls=%async_computation.6 | async-start | bytes 4194304 | tf_op jit(solution)/shard_map/all_to_all | solution.py:152
  140.0 0.7 copy.97
  140.7 29.8 %all-to-all-done.6 = bf16[64,8,2048]{2,1,0:T(8,128)(2,1)S(1)} async-done(((bf16[64,8,2048]{2,1,0:T(8,128)(2,1)}), bf16[64,8,2048]{2,1,0:T(8,128)(2,1)S(1)}, u32[]{:S(2)}, u32[]{:S(2)}) %all-to-all-start.6) | async-done | bytes 2097184 | tf_op jit(solution)/shard_map/all_to_all | solution.py:152
  170.4 1.4 gather_fusion.1
  171.8 0.7 reshape.219
  172.5 2.3 %multiply_reduce_fusion = f32[64,2048]{1,0:T(8,128)S(1)} fusion(f32[64,4,2048]{2,1,0:T(4,128)S(1)} %reshape.219, f32[64,4]{1,0:T(8,128)} %copy.97), kind=kLoop, calls=%fused_computation.17 | loop fusion | flops 917504 | bytes 2622464 | tf_op jit(solution)/shard_map/reduce_sum | solution.py:160
  174.8 0.8 fusion.30
  (48 shorter events, 1.7 us)
Async XLA Ops:
  0.0 37.2 %copy-start = (bf16[128,512]{1,0:T(8,128)(2,1)S(1)}, bf16[128,512]{1,0:T(8,128)(2,1)}, u32[]{:S(2)}) copy-start(bf16[128,512]{1,0:T(8,128)(2,1)} %param.13) | copy-start | bytes 393220
  0.0 37.0 %copy-start.3 = (bf16[128,1024]{1,0:T(8,128)(2,1)S(1)}, bf16[128,1024]{1,0:T(8,128)(2,1)}, u32[]{:S(2)}) copy-start(bf16[128,1024]{1,0:T(8,128)(2,1)} %param.16) | copy-start | bytes 786436
  7.0 42.8 %copy-start.2 = (bf16[128,1024]{1,0:T(8,128)(2,1)S(1)}, bf16[128,1024]{1,0:T(8,128)(2,1)}, u32[]{:S(2)}) copy-start(bf16[128,1024]{1,0:T(8,128)(2,1)} %param.15) | copy-start | bytes 786436
  7.0 22.3 %all-to-all-start = ((bf16[64,2,1024]{2,1,0:T(2,128)(2,1)}), bf16[64,2,1024]{2,1,0:T(2,128)(2,1)S(1)}, u32[]{:S(2)}, u32[]{:S(2)}) async-start(bf16[64,2,1024]{2,1,0:T(2,128)(2,1)} %reshape.251), calls=%async_computation | async-start | bytes 524288 | tf_op jit(solution)/shard_map/all_to_all | solution.py:28
  31.6 16.0 %all-to-all-start.1 = ((bf16[64,2,1024]{2,1,0:T(2,128)(2,1)}), bf16[64,2,1024]{2,1,0:T(2,128)(2,1)S(1)}, u32[]{:S(2)}, u32[]{:S(2)}) async-start(bf16[64,2,1024]{2,1,0:T(2,128)(2,1)} %reshape.253), calls=%async_computation.1 | async-start | bytes 524288 | tf_op jit(solution)/shard_map/all_to_all | solution.py:34
  50.7 7.4 %copy-start.4 = (bf16[64,2048]{1,0:T(8,128)(2,1)S(1)}, bf16[64,2048]{1,0:T(8,128)(2,1)}, u32[]{:S(2)}) copy-start(bf16[64,2048]{1,0:T(8,128)(2,1)} %param.18) | copy-start | bytes 786436
  50.9 7.4 %copy-start.5 = (f32[2048]{0:T(1024)S(1)}, f32[2048]{0:T(1024)}, u32[]{:S(2)}) copy-start(f32[2048]{0:T(1024)} %param.20) | copy-start | bytes 24580
  96.6 7.4 %copy-start.7 = (bf16[1,2048,1024]{2,1,0:T(8,128)(2,1)S(1)}, bf16[1,2048,1024]{2,1,0:T(8,128)(2,1)}, u32[]{:S(2)}) copy-start(bf16[1,2048,1024]{2,1,0:T(8,128)(2,1)} %param.24) | copy-start | bytes 12582916
  103.9 4.5 %copy-start.8 = (bf16[1,2048,1024]{2,1,0:T(8,128)(2,1)S(1)}, bf16[1,2048,1024]{2,1,0:T(8,128)(2,1)}, u32[]{:S(2)}) copy-start(bf16[1,2048,1024]{2,1,0:T(8,128)(2,1)} %param.23) | copy-start | bytes 12582916
  108.5 5.8 %copy-start.9 = (bf16[1,1024,2048]{2,1,0:T(8,128)(2,1)S(1)}, bf16[1,1024,2048]{2,1,0:T(8,128)(2,1)}, u32[]{:S(2)}) copy-start(bf16[1,1024,2048]{2,1,0:T(8,128)(2,1)} %param.25) | copy-start | bytes 12582916
  131.7 8.2 %copy-start.6 = (f32[64,4]{0,1:T(4,128)S(1)}, f32[64,4]{0,1:T(4,128)}, u32[]{:S(2)}) copy-start(f32[64,4]{0,1:T(4,128)} %param.22) | copy-start | bytes 3076
  134.3 36.2 %all-to-all-start.6 = ((bf16[64,8,2048]{2,1,0:T(8,128)(2,1)}), bf16[64,8,2048]{2,1,0:T(8,128)(2,1)S(1)}, u32[]{:S(2)}, u32[]{:S(2)}) async-start(bf16[64,8,2048]{2,1,0:T(8,128)(2,1)} %copy.96), calls=%async_computation.6 | async-start | bytes 4194304 | tf_op jit(solution)/shard_map/all_to_all | solution.py:152
  170.4 5.2 %copy-start.1 = (bf16[128,512]{1,0:T(8,128)(2,1)S(1)}, bf16[128,512]{1,0:T(8,128)(2,1)}, u32[]{:S(2)}) copy-start(bf16[128,512]{1,0:T(8,128)(2,1)} %param.13) | copy-start | bytes 393220
